TPU v7x, 32 devices: a whole 2x2x4 slice. The times are simulated.
32 devices in a mesh: grp: 2 (over y), fs: 4 (over z), tp: 4 (over x, core).
Axes of the slice: x: 2, y: 2, z: 4, core: 2. Of those that a mesh axis runs over, the one named last changes fastest.
Arguments:
- tokens: bfloat16 [2048, 2048], P(('grp', 'fs')), parts along dimension 0, may hold values from -6 to 6
- ffn_pre_gain: bfloat16 [2048], replicated, may hold values from 0.099609375 to 1.8984375
- gate_weight: bfloat16 [2048, 5632], P('fs', 'tp'), may hold values from -0.125 to 0.125
- up_weight: bfloat16 [2048, 5632], P('fs', 'tp'), may hold values from -0.125 to 0.125
- down_weight: bfloat16 [5632, 2048], P('tp', 'fs'), may hold values from -0.078125 to 0.078125
- ffn_post_gain: bfloat16 [2048], replicated, may hold values from 0.099609375 to 1.8984375
- mix_pre_gain: bfloat16 [2048], replicated, may hold values from 0.099609375 to 1.8984375
- mix_u_weight: bfloat16 [2048, 2048], P('fs', 'tp'), may hold values from -0.125 to 0.125
- mix_v_weight: bfloat16 [2048, 2048], P('fs', 'tp'), may hold values from -0.125 to 0.125
- spatial_gain: bfloat16 [2048], P('tp'), may hold values from 0.099609375 to 1.8984375
- spatial_weight: bfloat16 [16, 128, 128], P('tp'), may hold values from -0.5 to 0.5
- spatial_bias: bfloat16 [16, 128], P('tp'), may hold values from 0.099609375 to 1.8984375
- mix_out_weight: bfloat16 [2048, 2048], P('tp', 'fs'), may hold values from -0.125 to 0.125
- mix_post_gain: bfloat16 [2048], replicated, may hold values from 0.099609375 to 1.8984375
- late_pre_gain: bfloat16 [2048], replicated, may hold values from 0.099609375 to 1.8984375
- late_post_gain: bfloat16 [2048], replicated, may hold values from 0.099609375 to 1.8984375
Outputs:
- result: bfloat16 [2048, 2048], P(('grp', 'fs')), parts along dimension 0
There are 2 independent parts, one for each index of `grp`. A program takes and returns all parts, laid end to end along the dimension named above; an argument that names none is the same for every part. Nothing has to cross between parts.
All inputs are finite; a program needn't handle non-finite values.
Results may differ from a plain program's by a relative error of at most 0.019.
Values may be sent and summed in bfloat16 or wider, within the bound.
No kernel may reach another device: no remote copies, remote signals or barrier semaphores. Data moves between devices by JAX's collectives and lax.ppermute only.
A program may use at most 128 MiB of HBM per device.

v0:
```python
import jax
import jax.numpy as jnp
from jax import lax
from jax.sharding import PartitionSpec as P

GROUP_WIDTH = 128
BLOCK = 128


def row_norm(values, gain):
    scale = lax.rsqrt(jnp.mean(values * values, axis=-1, keepdims=True) + 1e-06)
    return values * scale * gain.astype(jnp.float32)


def reduce_partial(terms):
    return lax.psum(terms.astype(jnp.bfloat16), "tp").astype(jnp.float32)


def add_branch(stream, terms, gain, factor):
    total = reduce_partial(terms)
    return (stream.astype(jnp.float32) + factor * row_norm(total, gain)).astype(jnp.bfloat16)


def gated_hidden(normed, gate_full, up_full):
    gate = jnp.dot(normed, gate_full, preferred_element_type=jnp.float32)
    upper = jnp.dot(normed, up_full, preferred_element_type=jnp.float32)
    return (jax.nn.silu(gate) * upper).astype(jnp.bfloat16)


def spatial_mix(u_linear, v_linear, spatial_gain, spatial_weight, spatial_bias):
    count = u_linear.shape[0]
    gated_u = jax.nn.gelu(u_linear, approximate=False)
    gating_v = jax.nn.gelu(v_linear, approximate=False)
    groups = gating_v.shape[1] // GROUP_WIDTH
    grouped = gating_v.reshape(count, groups, GROUP_WIDTH)
    centred = grouped - jnp.mean(grouped, axis=-1, keepdims=True)
    vnorm = centred * lax.rsqrt(jnp.mean(centred * centred, axis=-1, keepdims=True) + 1e-05)
    vnorm = (vnorm * spatial_gain.astype(jnp.float32).reshape(groups, GROUP_WIDTH)).astype(
        jnp.bfloat16
    )
    blocks = vnorm.reshape(count // BLOCK, BLOCK, groups, GROUP_WIDTH)
    lower = jnp.tril(jnp.ones((BLOCK, BLOCK), dtype=bool))
    masked = jnp.where(lower[None], spatial_weight, jnp.zeros_like(spatial_weight))
    spatial = jnp.einsum("gts,nsgc->ntgc", masked, blocks, preferred_element_type=jnp.float32)
    spatial = spatial + spatial_bias.astype(jnp.float32).T[None, :, :, None]
    return (gated_u * spatial.reshape(count, groups * GROUP_WIDTH)).astype(jnp.bfloat16)


def shards(
    tokens,
    ffn_pre_gain,
    gate_weight,
    up_weight,
    down_weight,
    ffn_post_gain,
    mix_pre_gain,
    mix_u_weight,
    mix_v_weight,
    spatial_gain,
    spatial_weight,
    spatial_bias,
    mix_out_weight,
    mix_post_gain,
    late_pre_gain,
    late_post_gain,
):
    normed = row_norm(tokens.astype(jnp.float32), ffn_pre_gain).astype(jnp.bfloat16)
    gate_full, up_full = (
        lax.all_gather(gate_weight, "fs", axis=0, tiled=True),
        lax.all_gather(up_weight, "fs", axis=0, tiled=True),
    )
    down_full = lax.all_gather(down_weight, "fs", axis=1, tiled=True)
    hidden = gated_hidden(normed, gate_full, up_full)
    terms = jnp.dot(hidden, down_full, preferred_element_type=jnp.float32)
    first = add_branch(tokens, terms, ffn_post_gain, 0.5)
    normed = row_norm(first.astype(jnp.float32), mix_pre_gain).astype(jnp.bfloat16)
    u_full, v_full = (
        lax.all_gather(mix_u_weight, "fs", axis=0, tiled=True),
        lax.all_gather(mix_v_weight, "fs", axis=0, tiled=True),
    )
    u_linear = jnp.dot(normed, u_full, preferred_element_type=jnp.float32)
    v_linear = jnp.dot(normed, v_full, preferred_element_type=jnp.float32)
    mixed = spatial_mix(u_linear, v_linear, spatial_gain, spatial_weight, spatial_bias)
    out_full = lax.all_gather(mix_out_weight, "fs", axis=1, tiled=True)
    terms = jnp.dot(mixed, out_full, preferred_element_type=jnp.float32)
    second = add_branch(first, terms, mix_post_gain, 1.0)
    normed = row_norm(second.astype(jnp.float32), late_pre_gain).astype(jnp.bfloat16)
    hidden = gated_hidden(normed, gate_full, up_full)
    terms = jnp.dot(hidden, down_full, preferred_element_type=jnp.float32)
    return add_branch(second, terms, late_post_gain, 0.5)


def solution(mesh):
    in_specs = (
        P(("grp", "fs"), None),
        P(),
        P("fs", "tp"),
        P("fs", "tp"),
        P("tp", "fs"),
        P(),
        P(),
        P("fs", "tp"),
        P("fs", "tp"),
        P("tp"),
        P("tp", None, None),
        P("tp", None),
        P("tp", "fs"),
        P(),
        P(),
        P(),
    )
    out_specs = P(("grp", "fs"), None)
    return jax.shard_map(shards, mesh=mesh, in_specs=in_specs, out_specs=out_specs, check_vma=False)
```

profile of v0, /device:TPU:0, one launch (start us, length us, event | category | flops | bytes accessed | tf_op | source)
XLA Modules:
  0.0 620.2 jit_solution(5151979985591970159)
XLA Ops:
  6.5 0.7 all-gather.7.cloned.1.call-update
  7.3 0.0 all-gather.11.cloned.1.call-start
  7.3 0.7 all-gather.11.cloned.1.call-update
  8.0 0.0 all-gather.9.cloned.1.call-start
  8.1 0.7 all-gather.9.cloned.1.call-update
  8.7 0.0 all-reduce.4.cloned.1.call-start
  8.8 0.3 fusion.10
  9.1 109.2 %all-gather.7.cloned.1.call-done = bf16[2048,1408]{1,0:T(8,128)(2,1)} async-done(((bf16[512,1408]{1,0:T(8,128)(2,1)}), bf16[2048,1408]{1,0:T(8,128)(2,1)}) %all-gather.7.cloned.1.call-update) | async-done | bytes 5767184 | tf_op jit(solution)/shard_map/all_gather | solution.py:69
  118.3 4.5 fusion.59
  122.8 102.0 %all-gather.11.cloned.1.call-done = bf16[1408,2048]{1,0:T(8,128)(2,1)} async-done(((bf16[1408,512]{1,0:T(8,128)(2,1)}), bf16[1408,2048]{1,0:T(8,128)(2,1)}) %all-gather.11.cloned.1.call-update) | async-done | bytes 5767184 | tf_op jit(solution)/shard_map/all_gather | solution.py:72
  224.9 106.6 %all-gather.9.cloned.1.call-done = bf16[2048,1408]{1,0:T(8,128)(2,1)} async-done(((bf16[512,1408]{1,0:T(8,128)(2,1)}), bf16[2048,1408]{1,0:T(8,128)(2,1)}) %all-gather.9.cloned.1.call-update) | async-done | bytes 5767184 | tf_op jit(solution)/shard_map/all_gather | solution.py:70
  331.4 8.9 %convolution_convert_fusion.2 = bf16[256,2048]{1,0:T(8,128)(2,1)} fusion(bf16[1408,2048]{1,0:T(8,128)(2,1)} %all-gather.11.cloned.1.call-done, bf16[2048,1408]{1,0:T(8,128)(2,1)} %all-gather.9.cloned.1.call-done, f32[256,1408]{1,0:T(8,128)S(1)} %fusion.59, bf16[256,2048]{1,0:T(8,128)(2,1)S(1)} %copy-done, f32[2048]{0:T(1024)S(1)} %convert_element_type.82, ...), kind=kOutput, calls=%fused_computation.21 | convolution fusion | flops 2957574144 | bytes 15082496 | tf_op jit(solution)/shard_map/dot_general | solution.py:74
  340.4 0.0 all-reduce.4.cloned.1.call-update
  340.4 0.0 all-gather.15.cloned.1.call-start
  340.5 0.5 all-gather.15.cloned.1.call-update
  341.0 0.0 all-gather.13.cloned.1.call-start
  341.0 0.5 all-gather.13.cloned.1.call-update
  341.6 0.0 all-gather.17.cloned.1.call-start
  341.6 0.7 all-gather.17.cloned.1.call-update
  342.3 0.2 all-reduce.6.cloned.1.call-start
  342.7 32.4 %all-reduce.4.cloned.1.call-done = bf16[256,2048]{1,0:T(8,128)(2,1)} async-done(((bf16[256,2048]{1,0:T(8,128)(2,1)}), bf16[256,2048]{1,0:T(8,128)(2,1)}) %all-reduce.4.cloned.1.call-update) | async-done | bytes 1048592 | tf_op jit(solution)/shard_map/psum | solution.py:16
  375.1 1.5 fusion.2
  376.6 2.0 fusion.14
  378.6 44.1 %all-gather.15.cloned.1.call-done = bf16[2048,512]{1,0:T(8,128)(2,1)} async-done(((bf16[512,512]{1,0:T(8,128)(2,1)}), bf16[2048,512]{1,0:T(8,128)(2,1)}) %all-gather.15.cloned.1.call-update) | async-done | bytes 2097168 | tf_op jit(solution)/shard_map/all_gather | solution.py:79
  422.7 3.4 fusion.28
  426.1 0.2 reshape.99
  426.3 0.2 reshape.98
  426.5 0.3 reduce_sum.75
  426.8 0.6 multiply_reduce_fusion
  427.5 0.1 copy.36
  427.6 0.1 copy.37
  427.7 0.2 copy.25
  427.9 0.3 fusion.22
  428.2 0.2 copy.28
  428.5 40.1 %all-gather.13.cloned.1.call-done = bf16[2048,512]{1,0:T(8,128)(2,1)} async-done(((bf16[512,512]{1,0:T(8,128)(2,1)}), bf16[2048,512]{1,0:T(8,128)(2,1)}) %all-gather.13.cloned.1.call-update) | async-done | bytes 2097168 | tf_op jit(solution)/shard_map/all_gather | solution.py:78
  468.6 46.1 %all-gather.17.cloned.1.call-done = bf16[512,2048]{1,0:T(8,128)(2,1)} async-done(((bf16[512,512]{1,0:T(8,128)(2,1)}), bf16[512,2048]{1,0:T(8,128)(2,1)}) %all-gather.17.cloned.1.call-update) | async-done | bytes 2097168 | tf_op jit(solution)/shard_map/all_gather | solution.py:84
  514.7 5.7 convolution_convert_fusion
  520.4 0.0 all-reduce.6.cloned.1.call-update
  520.4 0.3 all-reduce.8.cloned.1.call-start
  520.7 34.9 %all-reduce.6.cloned.1.call-done = bf16[256,2048]{1,0:T(8,128)(2,1)} async-done(((bf16[256,2048]{1,0:T(8,128)(2,1)}), bf16[256,2048]{1,0:T(8,128)(2,1)}) %all-reduce.6.cloned.1.call-update) | async-done | bytes 1048592 | tf_op jit(solution)/shard_map/psum | solution.py:16
  555.7 1.5 fusion.5
  557.2 1.9 fusion.18
  559.1 4.5 fusion.45
  563.6 8.9 %convolution_convert_fusion.1 = bf16[256,2048]{1,0:T(8,128)(2,1)} fusion(bf16[1408,2048]{1,0:T(8,128)(2,1)} %all-gather.11.cloned.1.call-done, bf16[2048,1408]{1,0:T(8,128)(2,1)} %all-gather.9.cloned.1.call-done, f32[256,1408]{1,0:T(8,128)S(1)} %fusion.45, bf16[256,2048]{1,0:T(8,128)(2,1)S(1)} %get-tuple-element.6, f32[2048]{0:T(1024)S(1)} %convert_element_type.99, ...), kind=kOutput, calls=%fused_computation.20 | convolution fusion | flops 2957574144 | bytes 15082496 | tf_op jit(solution)/shard_map/dot_general | solution.py:89
  572.5 0.0 all-reduce.8.cloned.1.call-update
  572.5 36.9 %all-reduce.8.cloned.1.call-done = bf16[256,2048]{1,0:T(8,128)(2,1)} async-done(((bf16[256,2048]{1,0:T(8,128)(2,1)}), bf16[256,2048]{1,0:T(8,128)(2,1)}) %all-reduce.8.cloned.1.call-update) | async-done | bytes 1048592 | tf_op jit(solution)/shard_map/psum | solution.py:16
  609.4 1.5 fusion.7
  610.9 2.8 fusion.21
  (38 shorter events, 0.2 us)
Async XLA Ops:
  6.5 2.3 copy-start.2
  6.5 2.3 copy-start
  6.5 111.8 %all-gather.7.cloned.1.call-start = ((), (), s32[]{:S(2)}) async-start(), calls=%async_computation | async-start | bytes 7208960 | tf_op jit(solution)/shard_map/all_gather | solution.py:69
  7.3 217.6 %all-gather.11.cloned.1.call-start = ((), (), s32[]{:S(2)}) async-start(), calls=%async_computation.2 | async-start | bytes 7208960 | tf_op jit(solution)/shard_map/all_gather | solution.py:72
  8.0 323.4 %all-gather.9.cloned.1.call-start = ((), (), s32[]{:S(2)}) async-start(), calls=%async_computation.1 | async-start | bytes 7208960 | tf_op jit(solution)/shard_map/all_gather | solution.py:70
  8.7 366.4 %all-reduce.4.cloned.1.call-start = ((), (), s32[]{:S(2)}) async-start(), calls=%async_computation.3 | async-start | bytes 2097152 | tf_op jit(solution)/shard_map/psum | solution.py:16
  340.4 2.2 copy-start.3
  340.4 2.2 copy-start.4
  340.4 2.2 copy-start.8
  340.4 2.3 copy-start.9
  340.4 82.3 %all-gather.15.cloned.1.call-start = ((), (), s32[]{:S(2)}) async-start(), calls=%async_computation.5 | async-start | bytes 2621440 | tf_op jit(solution)/shard_map/all_gather | solution.py:79
  341.0 127.6 %all-gather.13.cloned.1.call-start = ((), (), s32[]{:S(2)}) async-start(), calls=%async_computation.4 | async-start | bytes 2621440 | tf_op jit(solution)/shard_map/all_gather | solution.py:78
  341.6 173.1 %all-gather.17.cloned.1.call-start = ((), (), s32[]{:S(2)}) async-start(), calls=%async_computation.6 | async-start | bytes 2621440 | tf_op jit(solution)/shard_map/all_gather | solution.py:84
  342.3 213.3 %all-reduce.6.cloned.1.call-start = ((), (), s32[]{:S(2)}) async-start(), calls=%async_computation.7 | async-start | bytes 2097152 | tf_op jit(solution)/shard_map/psum | solution.py:16
  426.3 1.7 copy-start.1
  514.7 6.0 copy-start.5
  514.7 6.0 copy-start.6
  520.4 89.0 %all-reduce.8.cloned.1.call-start = ((), (), s32[]{:S(2)}) async-start(), calls=%async_computation.8 | async-start | bytes 2097152 | tf_op jit(solution)/shard_map/psum | solution.py:16
  563.6 9.0 %copy-start.7 = (bf16[2048]{0:T(1024)(128)(2,1)S(1)}, bf16[2048]{0:T(1024)(128)(2,1)}, u32[]{:S(2)}) copy-start(bf16[2048]{0:T(1024)(128)(2,1)} %param.31) | copy-start | bytes 12292
Sparse Core Ops, SparseCore 0:
  8.9 109.3 all-gather.6
  119.9 104.9 all-gather.10
  226.5 104.9 all-gather.8
  340.5 34.5 all-reduce.3
  376.5 46.1 all-gather.14
  424.1 44.4 all-gather.12
  470.2 44.4 all-gather.16
  520.5 35.0 all-reduce.5
  572.6 36.7 all-reduce.7
where the time goes:
time: 621 us; the launch traced here: 620 us
  waiting for transfers between devices  556 us (90%)
  matrix products  36.2 us (6%)
  between operations  13.5 us (2%)
  other arithmetic  12.6 us (2%)
    all_gather x1, waiting for transfers between devices, shards(): lax.all_gather(gate_weight, 'fs', axis=0, tiled=True)  109 us
    all_gather x1, waiting for transfers between devices, shards(): lax.all_gather(up_weight, 'fs', axis=0, tiled=True)  107 us
    psum x3, waiting for transfers between devices, reduce_partial(): return lax.psum(terms.astype(jnp.bfloat16), 'tp').astype(jnp.float32)  104 us
    all_gather x1, waiting for transfers between devices, shards(): down_full = lax.all_gather(down_weight, 'fs', axis=1, tiled=True)  102 us
    all_gather x1, waiting for transfers between devices, shards(): out_full = lax.all_gather(mix_out_weight, 'fs', axis=1, tiled=True)  46.1 us
    all_gather x1, waiting for transfers between devices, shards(): lax.all_gather(mix_v_weight, 'fs', axis=0, tiled=True)  44.1 us
    all_gather x1, waiting for transfers between devices, shards(): lax.all_gather(mix_u_weight, 'fs', axis=0, tiled=True)  40.1 us
    dot_general x2, matrix products, shards(): terms = jnp.dot(hidden, down_full, preferred_element_type=jnp.float32)  17.8 us
  transfers between devices with their start and end apart: 9, of which 9 were waited for; matrix products, arithmetic and copies ran while one was open for 2% of the time, Pallas kernels for 0%

commit v1 on v0

--- a/solution.py
+++ b/solution.py
@@ -69,7 +69,12 @@
         lax.all_gather(gate_weight, "fs", axis=0, tiled=True),
         lax.all_gather(up_weight, "fs", axis=0, tiled=True),
     )
-    down_full = lax.all_gather(down_weight, "fs", axis=1, tiled=True)
+    ring = [down_weight]
+    for hop in range(3):
+        ring.append(lax.ppermute(ring[-1], "fs", [(dev, (dev + 1) % 4) for dev in range(4)]))
+    down_full = jnp.roll(
+        jnp.concatenate(ring[::-1], axis=1), (lax.axis_index("fs") + 1) * ring[0].shape[1], axis=1
+    )
     hidden = gated_hidden(normed, gate_full, up_full)
     terms = jnp.dot(hidden, down_full, preferred_element_type=jnp.float32)
     first = add_branch(tokens, terms, ffn_post_gain, 0.5)

time: 621 us -> 585 us (0.942)
  waiting for transfers between devices: 556 us -> 459 us
  starting transfers between devices: 0.71 us -> 43 us
  local copies, waits for them, and re-layouts: 1.03 us -> 17.2 us
    ppermute x0 -> x3, waiting for transfers between devices: none -> 170 us  [shards(): lax.ppermute(ring[-1], 'fs', [(dev, (dev + 1) % 4) for dev in range(4)])]
    all_gather x1, waiting for transfers between devices: 109 us -> 0.01 us  [shards(): lax.all_gather(gate_weight, 'fs', axis=0, tiled=True)]
    all_gather x1 -> x0, waiting for transfers between devices: 102 us -> none  [shards(): down_full = lax.all_gather(down_weight, 'fs', axis=1, tiled=True)]
    all_gather x1, waiting for transfers between devices: 107 us -> 51.8 us  [shards(): lax.all_gather(up_weight, 'fs', axis=0, tiled=True)]
    ppermute x0 -> x3, starting transfers between devices: none -> 42.3 us  [shards(): lax.ppermute(ring[-1], 'fs', [(dev, (dev + 1) % 4) for dev in range(4)])]
    unnamed x20 -> x37, local copies, waits for them, and re-layouts: 0.04 us -> 15 us
  transfers between devices with their start and end apart: 9 -> 11, of which waited for: 9 -> 10; matrix products, arithmetic and copies ran while one was open for 2% -> 5% of each run, Pallas kernels for 0% -> 0%
where the time goes in v1:
time: 585 us; the launch traced here: 584 us
  waiting for transfers between devices  459 us (78%)
  starting transfers between devices  43 us (7%)
  matrix products  36.1 us (6%)
  local copies, waits for them, and re-layouts  17.2 us (3%)
  other arithmetic  14.9 us (3%)
  between operations  13.8 us (2%)
    ppermute x3, waiting for transfers between devices, shards(): lax.ppermute(ring[-1], 'fs', [(dev, (dev + 1) % 4) for dev in range(4)])  170 us
    psum x3, waiting for transfers between devices, reduce_partial(): return lax.psum(terms.astype(jnp.bfloat16), 'tp').astype(jnp.float32)  104 us
    all_gather x1, waiting for transfers between devices, shards(): lax.all_gather(up_weight, 'fs', axis=0, tiled=True)  51.8 us
    all_gather x1, waiting for transfers between devices, shards(): out_full = lax.all_gather(mix_out_weight, 'fs', axis=1, tiled=True)  45.9 us
    all_gather x1, waiting for transfers between devices, shards(): lax.all_gather(mix_v_weight, 'fs', axis=0, tiled=True)  44.1 us
    ppermute x3, starting transfers between devices, shards(): lax.ppermute(ring[-1], 'fs', [(dev, (dev + 1) % 4) for dev in range(4)])  42.3 us
    all_gather x1, waiting for transfers between devices, shards(): lax.all_gather(mix_u_weight, 'fs', axis=0, tiled=True)  40.1 us
    dot_general x2, matrix products, shards(): terms = jnp.dot(hidden, down_full, preferred_element_type=jnp.float32)  17.8 us
  transfers between devices with their start and end apart: 11, of which 10 were waited for; matrix products, arithmetic and copies ran while one was open for 5% of the time, Pallas kernels for 0%

profile of v1, /device:TPU:0, one launch (start us, length us, event | category | flops | bytes accessed | tf_op | source)
XLA Modules:
  0.0 584.5 jit_solution(8035746232281083722)
XLA Ops:
  6.5 0.7 all-gather.6.cloned.1.call-update
  7.3 0.7 all-gather.8.cloned.1.call-update
  8.1 3.1 collective-permute-start
  11.2 54.4 %collective-permute-done = bf16[1408,512]{1,0:T(8,128)(2,1)S(1)} collective-permute-done((bf16[1408,512]{1,0:T(8,128)(2,1)S(1)}, bf16[1408,512]{1,0:T(8,128)(2,1)S(1)}, u32[]{:S(2)}, u32[]{:S(2)}) %collective-permute-start) | collective-permute-done | bytes 1441824 | tf_op jit(solution)/shard_map/ppermute | solution.py:74
  65.5 23.7 %collective-permute-start.1 = (bf16[1408,512]{1,0:T(8,128)(2,1)S(1)}, bf16[1408,512]{1,0:T(8,128)(2,1)}, u32[]{:S(2)}, u32[]{:S(2)}) collective-permute-start(bf16[1408,512]{1,0:T(8,128)(2,1)S(1)} %collective-permute-done), channel_id=1, source_target_pairs={{0,4},{4,8},{8,12},{12,0},{1,5},{5,9},{9,13},{13,1},{2,6},{6,10},{... | collective-permute-start | bytes 4325384 | tf_op jit(solution)/shard_map/ppermute | solution.py:74
  89.3 62.4 %collective-permute-done.1 = bf16[1408,512]{1,0:T(8,128)(2,1)} collective-permute-done((bf16[1408,512]{1,0:T(8,128)(2,1)S(1)}, bf16[1408,512]{1,0:T(8,128)(2,1)}, u32[]{:S(2)}, u32[]{:S(2)}) %collective-permute-start.1) | collective-permute-done | bytes 1441824 | tf_op jit(solution)/shard_map/ppermute | solution.py:74
  151.7 15.5 %collective-permute-start.2 = (bf16[1408,512]{1,0:T(8,128)(2,1)}, bf16[1408,512]{1,0:T(8,128)(2,1)}, u32[]{:S(2)}, u32[]{:S(2)}) collective-permute-start(bf16[1408,512]{1,0:T(8,128)(2,1)} %collective-permute-done.1), channel_id=1, source_target_pairs={{0,4},{4,8},{8,12},{12,0},{1,5},{5,9},{9,13},{13,1},{2,6},{6,10},{... | collective-permute-start | bytes 4325384 | tf_op jit(solution)/shard_map/ppermute | solution.py:74
  167.2 1.5 fusion.20
  168.7 53.5 %collective-permute-done.2 = bf16[1408,512]{1,0:T(8,128)(2,1)} collective-permute-done((bf16[1408,512]{1,0:T(8,128)(2,1)}, bf16[1408,512]{1,0:T(8,128)(2,1)}, u32[]{:S(2)}, u32[]{:S(2)}) %collective-permute-start.2) | collective-permute-done | bytes 1441824 | tf_op jit(solution)/shard_map/ppermute | solution.py:74
  222.2 2.7 constant_dynamic-update-slice_fusion.7
  224.9 2.7 constant_dynamic-update-slice_fusion.6
  227.5 1.2 constant_dynamic-update-slice_fusion.5
  228.8 1.3 constant_dynamic-update-slice_fusion.4
  230.0 2.7 constant_dynamic-update-slice_fusion.3
  232.7 2.6 constant_dynamic-update-slice_fusion.2
  235.4 1.3 constant_dynamic-update-slice_fusion.1
  236.7 1.3 constant_dynamic-update-slice_fusion
  238.0 0.5 copy-done.1
  238.4 4.5 fusion.69
  242.9 51.8 %all-gather.8.cloned.1.call-done = bf16[2048,1408]{1,0:T(8,128)(2,1)} async-done(((bf16[512,1408]{1,0:T(8,128)(2,1)}), bf16[2048,1408]{1,0:T(8,128)(2,1)}) %all-gather.8.cloned.1.call-update) | async-done | bytes 5767184 | tf_op jit(solution)/shard_map/all_gather | solution.py:70
  294.7 8.8 %fusion.6 = bf16[256,2048]{1,0:T(8,128)(2,1)} fusion(bf16[1408,4096]{1,0:T(8,128)(2,1)} %constant_dynamic-update-slice_fusion, s32[]{:T(128)S(6)} %select_n.20, bf16[2048,1408]{1,0:T(8,128)(2,1)} %all-gather.8.cloned.1.call-done, f32[256,1408]{1,0:T(8,128)S(1)} %fusion.69, bf16[256,2048]{1,0:T(8,128)(2,1)S(1)} %copy-done.1, ...), kind=kOutput, calls=%fused_computation.24 | convolution fusion | flops 2957574144 | bytes 15082500 | tf_op jit(solution)/shard_map/dot_general | solution.py:79
  303.6 0.5 all-gather.12.cloned.1.call-update
  304.2 0.5 all-gather.10.cloned.1.call-update
  304.8 0.5 all-gather.14.cloned.1.call-update
  305.7 0.6 bitcast_convert_fusion
  306.2 0.6 convert_bitcast_fusion
  306.8 32.3 %all-reduce.4.cloned.1.call-done = bf16[256,2048]{1,0:T(8,128)(2,1)} async-done(((bf16[256,2048]{1,0:T(8,128)(2,1)}), bf16[256,2048]{1,0:T(8,128)(2,1)}) %all-reduce.4.cloned.1.call-update) | async-done | bytes 1048592 | tf_op jit(solution)/shard_map/psum | solution.py:16
  339.1 1.5 fusion.12
  340.6 2.0 fusion.24
  342.6 44.1 %all-gather.12.cloned.1.call-done = bf16[2048,512]{1,0:T(8,128)(2,1)} async-done(((bf16[512,512]{1,0:T(8,128)(2,1)}), bf16[2048,512]{1,0:T(8,128)(2,1)}) %all-gather.12.cloned.1.call-update) | async-done | bytes 2097168 | tf_op jit(solution)/shard_map/all_gather | solution.py:84
  386.7 3.4 fusion.38
  390.5 0.3 reduce_sum.75
  390.9 0.6 multiply_reduce_fusion
  391.6 0.2 copy.25
  391.9 0.3 fusion.32
  392.2 0.2 copy.28
  392.5 40.1 %all-gather.10.cloned.1.call-done = bf16[2048,512]{1,0:T(8,128)(2,1)} async-done(((bf16[512,512]{1,0:T(8,128)(2,1)}), bf16[2048,512]{1,0:T(8,128)(2,1)}) %all-gather.10.cloned.1.call-update) | async-done | bytes 2097168 | tf_op jit(solution)/shard_map/all_gather | solution.py:83
  432.6 45.9 %all-gather.14.cloned.1.call-done = bf16[512,2048]{1,0:T(8,128)(2,1)} async-done(((bf16[512,512]{1,0:T(8,128)(2,1)}), bf16[512,2048]{1,0:T(8,128)(2,1)}) %all-gather.14.cloned.1.call-update) | async-done | bytes 2097168 | tf_op jit(solution)/shard_map/all_gather | solution.py:89
  478.5 5.7 convolution_convert_fusion
  484.3 0.3 all-reduce.8.cloned.1.call-start
  484.6 35.0 %all-reduce.6.cloned.1.call-done = bf16[256,2048]{1,0:T(8,128)(2,1)} async-done(((bf16[256,2048]{1,0:T(8,128)(2,1)}), bf16[256,2048]{1,0:T(8,128)(2,1)}) %all-reduce.6.cloned.1.call-update) | async-done | bytes 1048592 | tf_op jit(solution)/shard_map/psum | solution.py:16
  519.5 1.5 fusion.15
  521.1 1.9 fusion.28
  522.9 4.5 fusion.55
  527.5 9.0 %fusion.9 = bf16[256,2048]{1,0:T(8,128)(2,1)} fusion(bf16[1408,4096]{1,0:T(8,128)(2,1)} %constant_dynamic-update-slice_fusion, s32[]{:T(128)S(6)} %select_n.20, bf16[2048,1408]{1,0:T(8,128)(2,1)} %all-gather.8.cloned.1.call-done, f32[256,1408]{1,0:T(8,128)S(1)} %fusion.55, bf16[256,2048]{1,0:T(8,128)(2,1)S(1)} %get-tuple-element.6, ...), kind=kOutput, calls=%fused_computation.25 | convolution fusion | flops 2957574144 | bytes 15082500 | tf_op jit(solution)/shard_map/dot_general | solution.py:94
  536.5 36.9 %all-reduce.8.cloned.1.call-done = bf16[256,2048]{1,0:T(8,128)(2,1)} async-done(((bf16[256,2048]{1,0:T(8,128)(2,1)}), bf16[256,2048]{1,0:T(8,128)(2,1)}) %all-reduce.8.cloned.1.call-update) | async-done | bytes 1048592 | tf_op jit(solution)/shard_map/psum | solution.py:16
  573.4 1.5 fusion.17
  574.9 2.8 fusion.31
  (59 shorter events, 1.2 us)
Async XLA Ops:
  6.5 1.5 copy-start
  6.5 160.6 %copy-start.7 = (bf16[2048]{0:T(1024)(128)(2,1)S(1)}, bf16[2048]{0:T(1024)(128)(2,1)}, u32[]{:S(2)}) copy-start(bf16[2048]{0:T(1024)(128)(2,1)} %param.17) | copy-start | bytes 12292
  6.5 231.4 %all-gather.6.cloned.1.call-start = ((), (), s32[]{:S(2)}) async-start(), calls=%async_computation | async-start | bytes 7208960 | tf_op jit(solution)/shard_map/all_gather | solution.py:69
  7.3 287.5 %all-gather.8.cloned.1.call-start = ((), (), s32[]{:S(2)}) async-start(), calls=%async_computation.1 | async-start | bytes 7208960 | tf_op jit(solution)/shard_map/all_gather | solution.py:70
  8.0 331.1 %all-reduce.4.cloned.1.call-start = ((), (), s32[]{:S(2)}) async-start(), calls=%async_computation.2 | async-start | bytes 2097152 | tf_op jit(solution)/shard_map/psum | solution.py:16
  8.1 57.5 %collective-permute-start = (bf16[1408,512]{1,0:T(8,128)(2,1)S(1)}, bf16[1408,512]{1,0:T(8,128)(2,1)S(1)}, u32[]{:S(2)}, u32[]{:S(2)}) collective-permute-start(bf16[1408,512]{1,0:T(8,128)(2,1)S(1)} %copy-done), channel_id=1, source_target_pairs={{0,4},{4,8},{8,12},{12,0},{1,5},{5,9},{9,13},{13,1},{2,6},{6,10},{... | collective-permute-start | bytes 4325384 | tf_op jit(solution)/shard_map/ppermute | solution.py:74
  65.5 86.2 %collective-permute-start.1 = (bf16[1408,512]{1,0:T(8,128)(2,1)S(1)}, bf16[1408,512]{1,0:T(8,128)(2,1)}, u32[]{:S(2)}, u32[]{:S(2)}) collective-permute-start(bf16[1408,512]{1,0:T(8,128)(2,1)S(1)} %collective-permute-done), channel_id=1, source_target_pairs={{0,4},{4,8},{8,12},{12,0},{1,5},{5,9},{9,13},{13,1},{2,6},{6,10},{... | collective-permute-start | bytes 4325384 | tf_op jit(solution)/shard_map/ppermute | solution.py:74
  151.7 70.5 %collective-permute-start.2 = (bf16[1408,512]{1,0:T(8,128)(2,1)}, bf16[1408,512]{1,0:T(8,128)(2,1)}, u32[]{:S(2)}, u32[]{:S(2)}) collective-permute-start(bf16[1408,512]{1,0:T(8,128)(2,1)} %collective-permute-done.1), channel_id=1, source_target_pairs={{0,4},{4,8},{8,12},{12,0},{1,5},{5,9},{9,13},{13,1},{2,6},{6,10},{... | collective-permute-start | bytes 4325384 | tf_op jit(solution)/shard_map/ppermute | solution.py:74
  236.7 1.8 copy-start.1
  303.6 2.0 copy-start.8
  303.6 2.0 copy-start.9
  303.6 2.1 copy-start.13
  303.6 2.7 copy-start.14
  303.6 83.1 %all-gather.12.cloned.1.call-start = ((), (), s32[]{:S(2)}) async-start(), calls=%async_computation.4 | async-start | bytes 2621440 | tf_op jit(solution)/shard_map/all_gather | solution.py:84
  304.2 128.4 %all-gather.10.cloned.1.call-start = ((), (), s32[]{:S(2)}) async-start(), calls=%async_computation.3 | async-start | bytes 2621440 | tf_op jit(solution)/shard_map/all_gather | solution.py:83
  304.8 173.8 %all-gather.14.cloned.1.call-start = ((), (), s32[]{:S(2)}) async-start(), calls=%async_computation.5 | async-start | bytes 2621440 | tf_op jit(solution)/shard_map/all_gather | solution.py:89
  305.3 214.2 %all-reduce.6.cloned.1.call-start = ((), (), s32[]{:S(2)}) async-start(), calls=%async_computation.6 | async-start | bytes 2097152 | tf_op jit(solution)/shard_map/psum | solution.py:16
  305.6 81.1 %copy-start.5 = (f32[2048]{0:T(1024)}, f32[2048]{0:T(1024)S(1)}, u32[]{:S(2)}) copy-start(f32[2048]{0:T(1024)S(1)} %convert_element_type.90) | copy-start | bytes 24580
  390.3 1.7 copy-start.2
  390.3 1.7 copy-start.3
  390.3 1.6 copy-start.4
  391.5 87.0 %copy-start.6 = (f32[2048]{0:T(1024)S(1)}, f32[2048]{0:T(1024)}, u32[]{:S(2)}) copy-start(f32[2048]{0:T(1024)} %copy-done.5) | copy-start | bytes 24580
  478.5 6.0 %copy-start.10 = (bf16[2048]{0:T(1024)(128)(2,1)S(1)}, bf16[2048]{0:T(1024)(128)(2,1)}, u32[]{:S(2)}) copy-start(bf16[2048]{0:T(1024)(128)(2,1)} %param.29) | copy-start | bytes 12292
  478.5 6.0 %copy-start.11 = (bf16[2048]{0:T(1024)(128)(2,1)S(1)}, bf16[2048]{0:T(1024)(128)(2,1)}, u32[]{:S(2)}) copy-start(bf16[2048]{0:T(1024)(128)(2,1)} %param.30) | copy-start | bytes 12292
  484.3 89.1 %all-reduce.8.cloned.1.call-start = ((), (), s32[]{:S(2)}) async-start(), calls=%async_computation.7 | async-start | bytes 2097152 | tf_op jit(solution)/shard_map/psum | solution.py:16
  527.4 9.0 %copy-start.12 = (bf16[2048]{0:T(1024)(128)(2,1)S(1)}, bf16[2048]{0:T(1024)(128)(2,1)}, u32[]{:S(2)}) copy-start(bf16[2048]{0:T(1024)(128)(2,1)} %param.31) | copy-start | bytes 12292
Sparse Core Ops, SparseCore 0:
  8.9 159.9 all-gather.5
  170.5 124.1 all-gather.7
  303.7 35.3 all-reduce.3
  340.5 46.1 all-gather.11
  388.1 44.4 all-gather.9
  434.0 44.4 all-gather.13
  484.4 35.1 all-reduce.5
  536.6 36.7 all-reduce.7
